TPU v7x, 32 devices: a whole 2x2x4 slice. The times are simulated.
32 devices in a mesh: fs: 4 (over y, x), tp: 8 (over z, core).
Axes of the slice: x: 2, y: 2, z: 4, core: 2. Of those that a mesh axis runs over, the one named last changes fastest.
Arguments:
- tokens: bfloat16 [4096, 2048], P(('fs', 'tp')), may hold values from -6 to 6
- up_gate: bfloat16 [4096, 5632], P('fs', 'tp'), may hold values from -8 to 8
- up_val: bfloat16 [4096, 5632], P('fs', 'tp'), may hold values from -6 to 6
- gate_weight: bfloat16 [2048, 5632], P('fs', 'tp'), may hold values from -0.125 to 0.125
- val_weight: bfloat16 [2048, 5632], P('fs', 'tp'), may hold values from -0.125 to 0.125
- gate_taps: bfloat16 [3, 5632], P(None, 'tp'), may hold values from -3 to 3
- val_taps: bfloat16 [3, 5632], P(None, 'tp'), may hold values from -3 to 3
- hidden_grad: bfloat16 [4096, 5632], P('fs', 'tp'), may hold values from -6 to 6
Outputs:
- input_grad: bfloat16 [4096, 2048], P(('fs', 'tp'))
- gate_weight_grad: float32 [2048, 5632], P('fs', 'tp')
- val_weight_grad: float32 [2048, 5632], P('fs', 'tp')
- gate_taps_grad: float32 [3, 5632], P(None, 'tp')
- val_taps_grad: float32 [3, 5632], P(None, 'tp')
- gate_row_norms: float32 [2048], P('fs')
- val_row_norms: float32 [2048], P('fs')
- tap_row_norms: float32 [2, 3], replicated
All inputs are finite; a program needn't handle non-finite values.
Results may differ from a plain program's by a relative error of at most 0.017.
Values may be sent and summed in bfloat16 or wider, within the bound.
No kernel may reach another device: no remote copies, remote signals or barrier semaphores. Data moves between devices by JAX's collectives and lax.ppermute only.
A program may use at most 128 MiB of HBM per device.

v0:
```python
import jax
import jax.numpy as jnp
from jax import lax
from jax.sharding import PartitionSpec as P

SEQ = 1024


def shifted_sum(padded, kernel, length, backward):
    tap_count = kernel.shape[0]
    result = jnp.zeros((padded.shape[0], length, padded.shape[2]), jnp.float32)
    for tap_index in range(tap_count):
        tap_shift = tap_count - 1 - tap_index if backward else tap_index
        result = (
            result + kernel[tap_index][None, None, :] * padded[:, tap_shift : tap_shift + length]
        )
    return result


def local_grads(up_gate, up_val, hidden_grad, gate_taps, val_taps):
    length = up_gate.shape[1]
    tap_count = gate_taps.shape[0]
    gate_kernel = gate_taps.astype(jnp.float32)
    val_kernel = val_taps.astype(jnp.float32)
    pad_front = ((0, 0), (tap_count - 1, 0), (0, 0))
    pad_back = ((0, 0), (0, tap_count - 1), (0, 0))
    padded_gate = jnp.pad(up_gate.astype(jnp.float32), pad_front)
    padded_val = jnp.pad(up_val.astype(jnp.float32), pad_front)
    conv_gate = shifted_sum(padded_gate, gate_kernel, length, False)
    conv_val = shifted_sum(padded_val, val_kernel, length, False)
    sigmoid_gate = jax.nn.sigmoid(conv_gate)
    grad_hidden = hidden_grad.astype(jnp.float32)
    val_back = grad_hidden * conv_gate * sigmoid_gate
    gate_back = grad_hidden * conv_val * sigmoid_gate * (1.0 + conv_gate * (1.0 - sigmoid_gate))
    up_gate_back = shifted_sum(jnp.pad(gate_back, pad_back), gate_kernel, length, True).astype(
        jnp.bfloat16
    )
    up_val_back = shifted_sum(jnp.pad(val_back, pad_back), val_kernel, length, True).astype(
        jnp.bfloat16
    )
    tap_gate = jnp.stack(
        [
            jnp.sum(padded_gate[:, tap_index : tap_index + length] * gate_back, axis=(0, 1))
            for tap_index in range(tap_count)
        ]
    )
    tap_val = jnp.stack(
        [
            jnp.sum(padded_val[:, tap_index : tap_index + length] * val_back, axis=(0, 1))
            for tap_index in range(tap_count)
        ]
    )
    return (up_gate_back, up_val_back, tap_gate, tap_val)


def local(tokens, up_gate, up_val, gate_weight, val_weight, gate_taps, val_taps, hidden_grad):
    seq_count = up_gate.shape[0] // SEQ

    def as_blocks(values):
        return values.reshape(seq_count, SEQ, values.shape[1])

    gate_back, val_back, tap_gate, tap_val = local_grads(
        as_blocks(up_gate), as_blocks(up_val), as_blocks(hidden_grad), gate_taps, val_taps
    )
    gate_back = gate_back.reshape(up_gate.shape)
    val_back = val_back.reshape(up_val.shape)
    tap_gate, tap_val = lax.psum((tap_gate, tap_val), "fs")
    token_rows = lax.all_gather(tokens, "tp", axis=0, tiled=True)
    weight_contract = (((0,), (0,)), ((), ()))
    joined = jnp.concatenate((gate_back, val_back), axis=1)
    summed = lax.psum_scatter(
        lax.dot_general(
            token_rows, joined, weight_contract, preferred_element_type=jnp.float32
        ).astype(jnp.bfloat16),
        "fs",
        scatter_dimension=0,
        tiled=True,
    ).astype(jnp.float32)
    hidden_block = gate_back.shape[1]
    gate_grad = summed[:, :hidden_block]
    val_grad = summed[:, hidden_block:]
    gate_whole = lax.all_gather(gate_weight, "fs", axis=0, tiled=True)
    val_whole = lax.all_gather(val_weight, "fs", axis=0, tiled=True)
    contract = (((1,), (1,)), ((), ()))
    total = lax.dot_general(gate_back, gate_whole, contract, preferred_element_type=jnp.float32)
    input_grad = lax.psum_scatter(
        (
            total
            + lax.dot_general(val_back, val_whole, contract, preferred_element_type=jnp.float32)
        ).astype(jnp.bfloat16),
        "tp",
        scatter_dimension=0,
        tiled=True,
    )
    tap_squares = jnp.stack(
        [jnp.sum(tap_gate * tap_gate, axis=1), jnp.sum(tap_val * tap_val, axis=1)]
    )
    gate_norms, val_norms, tap_norms = lax.psum(
        (jnp.sum(gate_grad * gate_grad, axis=1), jnp.sum(val_grad * val_grad, axis=1), tap_squares),
        "tp",
    )
    return (input_grad, gate_grad, val_grad, tap_gate, tap_val, gate_norms, val_norms, tap_norms)


def solution(mesh):
    in_specs = (
        P(("fs", "tp"), None),
        P("fs", "tp"),
        P("fs", "tp"),
        P("fs", "tp"),
        P("fs", "tp"),
        P(None, "tp"),
        P(None, "tp"),
        P("fs", "tp"),
    )
    out_specs = (
        P(("fs", "tp"), None),
        P("fs", "tp"),
        P("fs", "tp"),
        P(None, "tp"),
        P(None, "tp"),
        P("fs"),
        P("fs"),
        P(),
    )
    return jax.shard_map(local, mesh=mesh, in_specs=in_specs, out_specs=out_specs, check_vma=False)
```

profile of v0, /device:TPU:0, one launch (start us, length us, event | category | flops | bytes accessed | tf_op | source)
XLA Modules:
  0.0 274.1 jit_solution(9604628618854611853)
XLA Ops:
  7.2 0.0 copy-start
  7.2 0.0 all-gather.8.cloned.1.call-start
  7.2 0.7 all-gather.8.cloned.1.call-update
  7.9 0.0 copy-start.5
  7.9 0.0 copy-start.1
  7.9 0.0 all-gather.4.cloned.1.call-start
  8.0 0.7 all-gather.4.cloned.1.call-update
  8.7 0.0 all-gather.6.cloned.1.call-start
  8.7 0.7 all-gather.6.cloned.1.call-update
  9.4 0.0 reduce-scatter.5.cloned.1.call-start
  9.5 0.0 copy-done
  9.5 0.3 convert_bitcast_fusion.1
  9.8 0.0 copy-done.5
  9.8 0.0 copy-start.6
  9.8 0.0 copy-start.2
  9.9 0.0 copy-done.1
  9.9 0.4 convert_bitcast_fusion
  10.3 0.2 copy-done.6
  10.6 0.6 copy-done.2
  11.2 10.8 %multiply_reduce_fusion.2 = (f32[704]{0:T(1024)S(1)}, f32[704]{0:T(1024)S(1)}, f32[704]{0:T(1024)S(1)}, f32[1,1024,704]{1,2,0:T(8,128)S(1)}, f32[704]{0:T(1024)S...) fusion(f32[1,1024,704]{1,2,0:T(8,128)S(1)} %convert_bitcast_fusion.1, ...), kind=kLoop, calls=%fused_computation.39 | loop fusion | flops 30994304 | bytes 15893504 | tf_op jit(solution)/shard_map/reduce_sum | solution.py:49
  22.1 4.9 %fusion.21 = (bf16[1024,704]{0,1:T(8,128)(2,1)S(1)}, bf16[1024,704]{0,1:T(8,128)(2,1)S(1)}) fusion(f32[1,1024,704]{1,2,0:T(8,128)S(1)} %get-tuple-element.29, f32[704]{0:T(1024)S(1)} %get-tuple-element.18, f32[704]{0:T(1024)S(1)} %get-tuple-element.19, f32[704]{0:T(1024)S(1)} %get-tuple-element.17, f32[1,1024,704]{1,2,0:T(8,128)S(1)} %get-tuple-element.34, ...), kind=kLoop, calls=%fused_computation.46 | loop fusion | flops 8650752 | bytes 8667648 | tf_op jit(solution)/shard_map/reshape | solution.py:66
  26.9 32.3 %all-gather.8.cloned.1.call-done = bf16[1024,2048]{1,0:T(8,128)(2,1)} async-done(((bf16[128,2048]{1,0:T(8,128)(2,1)}), bf16[1024,2048]{1,0:T(8,128)(2,1)}) %all-gather.8.cloned.1.call-update) | async-done | bytes 4194320 | tf_op jit(solution)/shard_map/all_gather | solution.py:68
  59.2 11.4 %fusion = bf16[2048,1408]{0,1:T(8,128)(2,1)} fusion(bf16[1024,2048]{1,0:T(8,128)(2,1)} %all-gather.8.cloned.1.call-done, bf16[1024,704]{0,1:T(8,128)(2,1)S(1)} %get-tuple-element.37, bf16[1024,704]{0,1:T(8,128)(2,1)S(1)} %get-tuple-element.38), kind=kOutput, calls=%fused_computation.2 | convolution fusion | flops 5914230784 | bytes 12845056 | tf_op jit(solution)/shard_map/dot_general | solution.py:72
  70.6 0.0 reduce-scatter.5.cloned.1.call-update
  70.6 0.0 reduce-scatter.3.cloned.1.call-start
  70.7 30.7 %all-gather.4.cloned.1.call-done = bf16[2048,704]{0,1:T(8,128)(2,1)} async-done(((bf16[512,704]{0,1:T(8,128)(2,1)}), bf16[2048,704]{0,1:T(8,128)(2,1)}) %all-gather.4.cloned.1.call-update) | async-done | bytes 2883600 | tf_op jit(solution)/shard_map/all_gather | solution.py:82
  101.4 7.5 %fusion.26 = f32[1024,2048]{1,0:T(8,128)} fusion(bf16[1024,704]{0,1:T(8,128)(2,1)S(1)} %get-tuple-element.38, bf16[2048,704]{0,1:T(8,128)(2,1)} %all-gather.4.cloned.1.call-done), kind=kOutput, calls=%fused_computation.60 | convolution fusion | flops 2952790016 | bytes 12713984 | tf_op jit(solution)/shard_map/dot_general | solution.py:85
  108.9 35.9 %all-gather.6.cloned.1.call-done = bf16[2048,704]{0,1:T(8,128)(2,1)} async-done(((bf16[512,704]{0,1:T(8,128)(2,1)}), bf16[2048,704]{0,1:T(8,128)(2,1)}) %all-gather.6.cloned.1.call-update) | async-done | bytes 2883600 | tf_op jit(solution)/shard_map/all_gather | solution.py:83
  144.8 8.2 %add_convert_fusion = bf16[1024,2048]{1,0:T(8,128)(2,1)} fusion(f32[1024,2048]{1,0:T(8,128)} %fusion.26, bf16[1024,704]{0,1:T(8,128)(2,1)S(1)} %get-tuple-element.37, bf16[2048,704]{0,1:T(8,128)(2,1)} %all-gather.6.cloned.1.call-done), kind=kOutput, calls=%fused_computation | convolution fusion | flops 2956984320 | bytes 16908288 | tf_op jit(solution)/shard_map/dot_general | solution.py:89
  153.0 0.0 reduce-scatter.3.cloned.1.call-update
  153.1 16.9 %all-reduce.5 = (f32[3,704]{1,0:T(4,128)S(1)}, f32[3,704]{1,0:T(4,128)S(1)}) all-reduce(f32[3,704]{1,0:T(4,128)S(1)} %pad_maximum_fusion, f32[3,704]{1,0:T(4,128)S(1)} %pad_maximum_fusion.1), channel_id=1, replica_groups=mesh['fs'=4,'tp'=8] {'fs'}, use_global_device_ids=true, to_apply=%region_5.6 | all-reduce | flops 4224 | bytes 33792 | tf_op jit(solution)/shard_map/psum | solution.py:67
  170.1 0.0 copy-start.3
  170.1 0.0 copy-start.4
  170.1 0.1 multiply_reduce_fusion.8
  170.2 44.2 %reduce-scatter.5.cloned.1.call-done = bf16[512,1408]{0,1:T(8,128)(2,1)} async-done(((bf16[2048,1408]{0,1:T(8,128)(2,1)}), bf16[512,1408]{0,1:T(8,128)(2,1)}) %reduce-scatter.5.cloned.1.call-update) | async-done | bytes 1441808 | tf_op jit(solution)/shard_map/reduce_scatter | solution.py:71
  214.4 3.3 %multiply_reduce_fusion.6 = (f32[512]{0:T(512)S(1)}, f32[512,704]{0,1:T(8,128)}, f32[512]{0:T(512)S(1)}, f32[512,704]{0,1:T(8,128)}) fusion(bf16[512,1408]{0,1:T(8,128)(2,1)} %reduce-scatter.5.cloned.1.call-done), kind=kLoop, calls=%fused_computation.44 | loop fusion | flops 1440768 | bytes 5771264 | tf_op jit(solution)/shard_map/reduce_sum | solution.py:99
  217.8 0.0 copy-done.3
  217.8 0.0 copy-done.4
  217.8 17.5 %all-reduce.4 = (f32[512]{0:T(512)}, f32[512]{0:T(512)}, f32[2,3]{1,0:T(2,128)}) all-reduce(f32[512]{0:T(512)S(1)} %get-tuple-element.35, f32[512]{0:T(512)S(1)} %get-tuple-element.25, f32[2,3]{1,0:T(2,128)S(1)} %pad_maximum_fusion.2), channel_id=1, replica_groups=mesh['fs'=4,'tp'=8] {'tp'}, use_global_device_ids=true, to_apply=%region_11.12 | all-reduce | flops 1030 | bytes 8240 | tf_op jit(solution)/shard_map/psum | solution.py:98
  235.2 32.4 %reduce-scatter.3.cloned.1.call-done = bf16[128,2048]{1,0:T(8,128)(2,1)} async-done(((bf16[1024,2048]{1,0:T(8,128)(2,1)}), bf16[128,2048]{1,0:T(8,128)(2,1)}) %reduce-scatter.3.cloned.1.call-update) | async-done | bytes 524304 | tf_op jit(solution)/shard_map/reduce_scatter | solution.py:86
  (13 shorter events, 0.1 us)
Async XLA Ops:
  7.2 2.3 copy-start
  7.2 52.0 %all-gather.8.cloned.1.call-start = ((), (), s32[]{:S(2)}) async-start(), calls=%async_computation.5 | async-start | bytes 4718592 | tf_op jit(solution)/shard_map/all_gather | solution.py:68
  7.9 1.9 copy-start.5
  7.9 2.0 copy-start.1
  7.9 93.5 %all-gather.4.cloned.1.call-start = ((), (), s32[]{:S(2)}) async-start(), calls=%async_computation.2 | async-start | bytes 3604480 | tf_op jit(solution)/shard_map/all_gather | solution.py:82
  8.7 136.2 %all-gather.6.cloned.1.call-start = ((), (), s32[]{:S(2)}) async-start(), calls=%async_computation.3 | async-start | bytes 3604480 | tf_op jit(solution)/shard_map/all_gather | solution.py:83
  9.4 205.0 %reduce-scatter.5.cloned.1.call-start = ((), (), s32[]{:S(2)}) async-start(), calls=%async_computation.6 | async-start | bytes 7208960 | tf_op jit(solution)/shard_map/reduce_scatter | solution.py:71
  9.8 0.7 copy-start.6
  9.8 1.4 copy-start.2
  70.6 197.0 %reduce-scatter.3.cloned.1.call-start = ((), (), s32[]{:S(2)}) async-start(), calls=%async_computation.4 | async-start | bytes 4718592 | tf_op jit(solution)/shard_map/reduce_scatter | solution.py:86
  170.1 47.7 %copy-start.3 = (f32[3,704]{1,0:T(4,128)}, f32[3,704]{1,0:T(4,128)S(1)}, u32[]{:S(2)}) copy-start(f32[3,704]{1,0:T(4,128)S(1)} %get-tuple-element.23) | copy-start | bytes 25348
  170.1 47.7 %copy-start.4 = (f32[3,704]{1,0:T(4,128)}, f32[3,704]{1,0:T(4,128)S(1)}, u32[]{:S(2)}) copy-start(f32[3,704]{1,0:T(4,128)S(1)} %get-tuple-element.24) | copy-start | bytes 25348
Sparse Core Ops, SparseCore 0:
  9.6 49.5 all-gather.7
  61.0 40.3 all-gather.3
  103.3 41.5 all-gather.5
  147.7 66.6 reduce-scatter.4
  217.1 50.4 reduce-scatter.2
where the time goes:
time: 274 us
  waiting for transfers between devices  178 us (65%)
  blocking collectives  34.4 us (13%)
  matrix products  27 us (10%)
  other arithmetic  19.9 us (7%)
  between operations  14 us (5%)
    reduce_scatter x1, waiting for transfers between devices, local(): lax.psum_scatter(lax.dot_general(token_rows, joined, weight_contract, pre...  44.2 us
    all_gather x1, waiting for transfers between devices, local(): val_whole = lax.all_gather(val_weight, 'fs', axis=0, tiled=True)  35.9 us
    reduce_scatter x1, waiting for transfers between devices, local(): lax.psum_scatter((total + lax.dot_general(val_back, val_whole, contract,...  32.4 us
    all_gather x1, waiting for transfers between devices, local(): token_rows = lax.all_gather(tokens, 'tp', axis=0, tiled=True)  32.3 us
    all_gather x1, waiting for transfers between devices, local(): gate_whole = lax.all_gather(gate_weight, 'fs', axis=0, tiled=True)  30.7 us
    psum x1, blocking collectives, local(): lax.psum((jnp.sum(gate_grad * gate_grad, axis=1), jnp.sum(val_grad * val_...  17.5 us
    psum x1, blocking collectives, local(): tap_gate, tap_val = lax.psum((tap_gate, tap_val), 'fs')  16.9 us
    dot_general x1, matrix products, local(): lax.dot_general(token_rows, joined, weight_contract, preferred_element_ty...  11.4 us
  transfers between devices with their start and end apart: 5, of which 5 were waited for; matrix products, arithmetic and copies ran while one was open for 17% of the time, Pallas kernels for 0%

commit v1 on v0

--- a/solution.py
+++ b/solution.py
@@ -4,6 +4,21 @@
 from jax.sharding import PartitionSpec as P
 
 SEQ = 1024
+
+
+def move_edge_here(local_values, pos_dim):
+    n = lax.axis_size("fs")
+    seen = [local_values]
+    for dd in [*range(n - 1)]:
+        seen.append(
+            lax.ppermute(seen[-1], axis_name="fs", perm=[(d, (d + 1) % n) for d in range(n)])
+        )
+    piece_next = jnp.roll(
+        jnp.concatenate(seen[::-1], axis=pos_dim),
+        shift=(lax.axis_index("fs") + 1) * local_values.shape[pos_dim],
+        axis=pos_dim,
+    )
+    return piece_next
 
 
 def shifted_sum(padded, kernel, length, backward):
@@ -79,7 +94,7 @@
     hidden_block = gate_back.shape[1]
     gate_grad = summed[:, :hidden_block]
     val_grad = summed[:, hidden_block:]
-    gate_whole = lax.all_gather(gate_weight, "fs", axis=0, tiled=True)
+    gate_whole = move_edge_here(gate_weight, 0)
     val_whole = lax.all_gather(val_weight, "fs", axis=0, tiled=True)
     contract = (((1,), (1,)), ((), ()))
     total = lax.dot_general(gate_back, gate_whole, contract, preferred_element_type=jnp.float32)

time: 274 us -> 261 us (0.953)
  waiting for transfers between devices: 178 us -> 155 us
  local copies, waits for them, and re-layouts: 1 us -> 9.37 us
  other arithmetic: 19.9 us -> 23 us
    ppermute x0 -> x3, waiting for transfers between devices: none -> 84.1 us  [move_edge_here(): lax.ppermute(seen[-1], axis_name='fs', perm=[(d, (d + 1) % n) for d in ra...]
    reduce_scatter x1, waiting for transfers between devices: 44.2 us -> 6.77 us  [local(): lax.psum_scatter(lax.dot_general(token_rows, joined, weight_contract, pre...]
    all_gather x1, waiting for transfers between devices: 35.9 us -> 0.01 us  [local(): val_whole = lax.all_gather(val_weight, 'fs', axis=0, tiled=True)]
    all_gather x1 -> x0, waiting for transfers between devices: 30.7 us -> none  [local(): gate_whole = lax.all_gather(gate_weight, 'fs', axis=0, tiled=True)]
    unnamed x14 -> x25, local copies, waits for them, and re-layouts: 0.91 us -> 8.27 us
    reduce_sum x1 -> x2, other arithmetic: 10.8 us -> 11.1 us  [the longest x1 11 us: local_grads(): jnp.sum(padded_gate[:, tap_index:tap_index + length] * gate_back, axis=(0...]
  transfers between devices with their start and end apart: 5 -> 7, of which waited for: 5 -> 6; matrix products, arithmetic and copies ran while one was open for 17% -> 21% of each run, Pallas kernels for 0% -> 0%
where the time goes in v1:
time: 261 us; the launch traced here: 260 us
  waiting for transfers between devices  155 us (59%)
  blocking collectives  33.1 us (13%)
  matrix products  24.4 us (9%)
  other arithmetic  23 us (9%)
  between operations  14 us (5%)
  local copies, waits for them, and re-layouts  9.37 us (4%)
    ppermute x3, waiting for transfers between devices, move_edge_here(): lax.ppermute(seen[-1], axis_name='fs', perm=[(d, (d + 1) % n) for d in ra...  84.1 us
    reduce_scatter x1, waiting for transfers between devices, local(): lax.psum_scatter((total + lax.dot_general(val_back, val_whole, contract,...  32 us
    all_gather x1, waiting for transfers between devices, local(): token_rows = lax.all_gather(tokens, 'tp', axis=0, tiled=True)  30.6 us
    psum x1, blocking collectives, local(): lax.psum((jnp.sum(gate_grad * gate_grad, axis=1), jnp.sum(val_grad * val_...  17.7 us
    psum x1, blocking collectives, local(): tap_gate, tap_val = lax.psum((tap_gate, tap_val), 'fs')  15.4 us
    dot_general x1, matrix products, local(): lax.dot_general(token_rows, joined, weight_contract, preferred_element_ty...  11.4 us
    reduce_sum x1, other arithmetic, local_grads(): jnp.sum(padded_gate[:, tap_index:tap_index + length] * gate_back, axis=(0...  11 us
    unnamed x25, local copies, waits for them, and re-layouts  8.27 us
  transfers between devices with their start and end apart: 7, of which 6 were waited for; matrix products, arithmetic and copies ran while one was open for 21% of the time, Pallas kernels for 0%

profile of v1, /device:TPU:0, one launch (start us, length us, event | category | flops | bytes accessed | tf_op | source)
XLA Modules:
  0.0 260.3 jit_solution(6819455332922370535)
XLA Ops:
  7.2 0.0 all-gather.5.cloned.1.call-start
  7.2 0.7 all-gather.5.cloned.1.call-update
  7.9 0.0 all-gather.3.cloned.1.call-start
  7.9 0.7 all-gather.3.cloned.1.call-update
  8.7 0.0 reduce-scatter.5.cloned.1.call-start
  8.7 0.7 convert_element_type.48
  9.4 0.7 convert_element_type.51
  10.1 0.1 slice_reduce_fusion.4
  10.1 0.0 copy-start
  10.2 0.0 copy-start.1
  10.2 0.0 copy-start.6
  10.2 2.6 %convert_bitcast_fusion = (f32[1,1024,704]{1,2,0:T(8,128)S(1)}, f32[1,1024,704]{1,2,0:T(8,128)S(1)}) fusion(bf16[1024,704]{0,1:T(8,128)(2,1)} %param.9, bf16[1024,704]{0,1:T(8,128)(2,1)} %param.10), kind=kLoop, calls=%fused_computation.6 | loop fusion | flops 1441792 | bytes 8650752 | tf_op jit(solution)/shard_map/convert_element_type | solution.py:42
  12.8 0.4 copy-done.6
  13.3 11.0 %multiply_reduce_fusion.5 = (f32[704]{0:T(1024)S(1)}, f32[704]{0:T(1024)S(1)}, f32[704]{0:T(1024)S(1)}, f32[1,1024,704]{1,2,0:T(8,128)S(1)}, f32[704]{0:T(1024)S...) fusion(f32[1,1024,704]{1,2,0:T(8,128)S(1)} %get-tuple-element.37, ...), kind=kLoop, calls=%fused_computation.42 | loop fusion | flops 30994304 | bytes 15893504 | tf_op jit(solution)/shard_map/reduce_sum | solution.py:58
  24.2 2.2 fusion.23
  26.4 0.0 copy-start.3
  26.4 2.2 fusion.22
  28.6 0.0 copy-start.5
  28.6 30.6 %all-gather.5.cloned.1.call-done = bf16[1024,2048]{1,0:T(8,128)(2,1)} async-done(((bf16[128,2048]{1,0:T(8,128)(2,1)}), bf16[1024,2048]{1,0:T(8,128)(2,1)}) %all-gather.5.cloned.1.call-update) | async-done | bytes 4194320 | tf_op jit(solution)/shard_map/all_gather | solution.py:83
  59.2 11.4 %fusion = bf16[2048,1408]{0,1:T(8,128)(2,1)} fusion(bf16[1024,2048]{1,0:T(8,128)(2,1)} %all-gather.5.cloned.1.call-done, bf16[1024,704]{0,1:T(8,128)(2,1)S(1)} %fusion.22, bf16[1024,704]{0,1:T(8,128)(2,1)S(1)} %fusion.23), kind=kOutput, calls=%fused_computation.2 | convolution fusion | flops 5914230784 | bytes 12845056 | tf_op jit(solution)/shard_map/dot_general | solution.py:87
  70.6 0.0 reduce-scatter.5.cloned.1.call-update
  70.6 0.0 reduce-scatter.3.cloned.1.call-start
  70.7 1.0 copy-done.2
  71.7 1.5 collective-permute-start
  73.2 23.8 %collective-permute-done = bf16[512,704]{0,1:T(8,128)(2,1)S(1)} collective-permute-done((bf16[512,704]{0,1:T(8,128)(2,1)S(1)}, bf16[512,704]{0,1:T(8,128)(2,1)S(1)}, u32[]{:S(2)}, u32[]{:S(2)}) %collective-permute-start) | collective-permute-done | bytes 720928 | tf_op jit(solution)/shard_map/ppermute | solution.py:14
  97.0 0.0 collective-permute-start.1
  97.0 28.1 %collective-permute-done.1 = bf16[512,704]{0,1:T(8,128)(2,1)S(1)} collective-permute-done((bf16[512,704]{0,1:T(8,128)(2,1)S(1)}, bf16[512,704]{0,1:T(8,128)(2,1)S(1)}, u32[]{:S(2)}, u32[]{:S(2)}) %collective-permute-start.1) | collective-permute-done | bytes 720928 | tf_op jit(solution)/shard_map/ppermute | solution.py:14
  125.1 0.0 collective-permute-start.2
  125.1 32.2 %collective-permute-done.2 = bf16[512,704]{0,1:T(8,128)(2,1)S(1)} collective-permute-done((bf16[512,704]{0,1:T(8,128)(2,1)S(1)}, bf16[512,704]{0,1:T(8,128)(2,1)S(1)}, u32[]{:S(2)}, u32[]{:S(2)}) %collective-permute-start.2) | collective-permute-done | bytes 720928 | tf_op jit(solution)/shard_map/ppermute | solution.py:14
  157.3 1.0 constant_dynamic-update-slice_fusion.7
  158.3 1.0 constant_dynamic-update-slice_fusion.6
  159.2 0.9 constant_dynamic-update-slice_fusion.5
  160.2 0.9 constant_dynamic-update-slice_fusion.4
  161.1 1.0 constant_dynamic-update-slice_fusion.3
  162.1 1.0 constant_dynamic-update-slice_fusion.2
  163.1 1.0 constant_dynamic-update-slice_fusion.1
  164.1 1.0 constant_dynamic-update-slice_fusion
  165.1 5.9 %fusion.28 = f32[1024,2048]{1,0:T(8,128)S(1)} fusion(bf16[1024,704]{0,1:T(8,128)(2,1)} %copy-done.5, bf16[2048,704]{0,1:T(8,128)(2,1)} %all-gather.3.cloned.1.call-done), kind=kOutput, calls=%fused_computation.70 | convolution fusion | flops 2952790016 | bytes 12713984 | tf_op jit(solution)/shard_map/dot_general | solution.py:104
  171.0 7.2 %add_convert_fusion = bf16[1024,2048]{1,0:T(8,128)(2,1)} fusion(f32[1024,2048]{1,0:T(8,128)S(1)} %fusion.28, bf16[1024,704]{0,1:T(8,128)(2,1)S(1)} %copy-done.4, bf16[4096,704]{0,1:T(8,128)(2,1)} %constant_dynamic-update-slice_fusion, s32[]{:T(128)S(6)} %select_n.14), kind=kOutput, calls=%fused_computation | convolution fusion | flops 2956984320 | bytes 16908292 | tf_op jit(solution)/shard_map/dot_general | solution.py:100
  178.2 0.0 reduce-scatter.3.cloned.1.call-update
  178.3 15.4 %all-reduce.5 = (f32[3,704]{1,0:T(4,128)S(1)}, f32[3,704]{1,0:T(4,128)S(1)}) all-reduce(f32[3,704]{1,0:T(4,128)S(1)} %pad_maximum_fusion, f32[3,704]{1,0:T(4,128)S(1)} %pad_maximum_fusion.1), channel_id=1, replica_groups=mesh['fs'=4,'tp'=8] {'fs'}, use_global_device_ids=true, to_apply=%region_5.6 | all-reduce | flops 4224 | bytes 33792 | tf_op jit(solution)/shard_map/psum | solution.py:82
  193.7 0.0 copy-start.8
  193.7 0.1 multiply_reduce_fusion.9
  193.8 0.1 multiply_reduce_fusion.8
  193.9 6.8 %reduce-scatter.5.cloned.1.call-done = bf16[512,1408]{0,1:T(8,128)(2,1)} async-done(((bf16[2048,1408]{0,1:T(8,128)(2,1)}), bf16[512,1408]{0,1:T(8,128)(2,1)}) %reduce-scatter.5.cloned.1.call-update) | async-done | bytes 1441808 | tf_op jit(solution)/shard_map/reduce_scatter | solution.py:86
  200.7 3.3 %multiply_reduce_fusion.6 = (f32[512]{0:T(512)S(1)}, f32[512,704]{0,1:T(8,128)}, f32[512]{0:T(512)S(1)}, f32[512,704]{0,1:T(8,128)}) fusion(bf16[512,1408]{0,1:T(8,128)(2,1)} %reduce-scatter.5.cloned.1.call-done), kind=kLoop, calls=%fused_computation.45 | loop fusion | flops 1440768 | bytes 5771264 | tf_op jit(solution)/shard_map/reduce_sum | solution.py:114
  204.0 17.7 %all-reduce.4 = (f32[512]{0:T(512)}, f32[512]{0:T(512)}, f32[2,3]{1,0:T(2,128)}) all-reduce(f32[512]{0:T(512)S(1)} %get-tuple-element.35, f32[512]{0:T(512)S(1)} %get-tuple-element.25, f32[2,3]{1,0:T(2,128)S(1)} %pad_maximum_fusion.2), channel_id=1, replica_groups=mesh['fs'=4,'tp'=8] {'tp'}, use_global_device_ids=true, to_apply=%region_11.12 | all-reduce | flops 1030 | bytes 8240 | tf_op jit(solution)/shard_map/psum | solution.py:113
  221.8 32.0 %reduce-scatter.3.cloned.1.call-done = bf16[128,2048]{1,0:T(8,128)(2,1)} async-done(((bf16[1024,2048]{1,0:T(8,128)(2,1)}), bf16[128,2048]{1,0:T(8,128)(2,1)}) %reduce-scatter.3.cloned.1.call-update) | async-done | bytes 524304 | tf_op jit(solution)/shard_map/reduce_scatter | solution.py:101
  (20 shorter events, 0.1 us)
Async XLA Ops:
  7.2 52.0 %all-gather.5.cloned.1.call-start = ((), (), s32[]{:S(2)}) async-start(), calls=%async_computation.4 | async-start | bytes 4718592 | tf_op jit(solution)/shard_map/all_gather | solution.py:83
  7.9 157.2 %all-gather.3.cloned.1.call-start = ((), (), s32[]{:S(2)}) async-start(), calls=%async_computation.2 | async-start | bytes 3604480 | tf_op jit(solution)/shard_map/all_gather | solution.py:98
  8.7 192.1 %reduce-scatter.5.cloned.1.call-start = ((), (), s32[]{:S(2)}) async-start(), calls=%async_computation.5 | async-start | bytes 7208960 | tf_op jit(solution)/shard_map/reduce_scatter | solution.py:86
  10.1 2.7 %copy-start = (bf16[1024,704]{0,1:T(8,128)(2,1)S(1)}, bf16[1024,704]{0,1:T(8,128)(2,1)}, u32[]{:S(2)}) copy-start(bf16[1024,704]{0,1:T(8,128)(2,1)} %param.9) | copy-start | bytes 4325380
  10.2 2.7 %copy-start.1 = (bf16[1024,704]{0,1:T(8,128)(2,1)S(1)}, bf16[1024,704]{0,1:T(8,128)(2,1)}, u32[]{:S(2)}) copy-start(bf16[1024,704]{0,1:T(8,128)(2,1)} %param.10) | copy-start | bytes 4325380
  10.2 3.1 %copy-start.6 = (bf16[1024,704]{0,1:T(8,128)(2,1)S(1)}, bf16[1024,704]{0,1:T(8,128)(2,1)}, u32[]{:S(2)}) copy-start(bf16[1024,704]{0,1:T(8,128)(2,1)} %param.15) | copy-start | bytes 4325380
  26.4 44.1 %copy-start.3 = (bf16[1024,704]{0,1:T(8,128)(2,1)}, bf16[1024,704]{0,1:T(8,128)(2,1)S(1)}, u32[]{:S(2)}) copy-start(bf16[1024,704]{0,1:T(8,128)(2,1)S(1)} %fusion.23) | copy-start | bytes 4325380
  28.6 41.9 %copy-start.5 = (bf16[1024,704]{0,1:T(8,128)(2,1)}, bf16[1024,704]{0,1:T(8,128)(2,1)S(1)}, u32[]{:S(2)}) copy-start(bf16[1024,704]{0,1:T(8,128)(2,1)S(1)} %fusion.22) | copy-start | bytes 4325380
  70.6 1.1 copy-start.2
  70.6 183.2 %reduce-scatter.3.cloned.1.call-start = ((), (), s32[]{:S(2)}) async-start(), calls=%async_computation.3 | async-start | bytes 4718592 | tf_op jit(solution)/shard_map/reduce_scatter | solution.py:101
  71.7 25.3 %collective-permute-start = (bf16[512,704]{0,1:T(8,128)(2,1)S(1)}, bf16[512,704]{0,1:T(8,128)(2,1)S(1)}, u32[]{:S(2)}, u32[]{:S(2)}) collective-permute-start(bf16[512,704]{0,1:T(8,128)(2,1)S(1)} %copy-done.2), channel_id=1, source_target_pairs={{0,8},{8,16},{16,24},{24,0},{1,9},{9,17},{17,25},{25,1},{2,10},{10... | collective-permute-start | bytes 2162696 | tf_op jit(solution)/shard_map/ppermute | solution.py:14
  97.0 28.1 %collective-permute-start.1 = (bf16[512,704]{0,1:T(8,128)(2,1)S(1)}, bf16[512,704]{0,1:T(8,128)(2,1)S(1)}, u32[]{:S(2)}, u32[]{:S(2)}) collective-permute-start(bf16[512,704]{0,1:T(8,128)(2,1)S(1)} %collective-permute-done), channel_id=1, source_target_pairs={{0,8},{8,16},{16,24},{24,0},{1,9},{9,17},{17,25},{25,1},{2,10},{10... | collective-permute-start | bytes 2162696 | tf_op jit(solution)/shard_map/ppermute | solution.py:14
  125.1 32.2 %collective-permute-start.2 = (bf16[512,704]{0,1:T(8,128)(2,1)S(1)}, bf16[512,704]{0,1:T(8,128)(2,1)S(1)}, u32[]{:S(2)}, u32[]{:S(2)}) collective-permute-start(bf16[512,704]{0,1:T(8,128)(2,1)S(1)} %collective-permute-done.1), channel_id=1, source_target_pairs={{0,8},{8,16},{16,24},{24,0},{1,9},{9,17},{17,25},{25,1},{2,10},{10... | collective-permute-start | bytes 2162696 | tf_op jit(solution)/shard_map/ppermute | solution.py:14
  165.1 5.9 %copy-start.4 = (bf16[1024,704]{0,1:T(8,128)(2,1)S(1)}, bf16[1024,704]{0,1:T(8,128)(2,1)}, u32[]{:S(2)}) copy-start(bf16[1024,704]{0,1:T(8,128)(2,1)} %copy-done.3) | copy-start | bytes 4325380
  193.7 10.4 %copy-start.7 = (f32[3,704]{1,0:T(4,128)}, f32[3,704]{1,0:T(4,128)S(1)}, u32[]{:S(2)}) copy-start(f32[3,704]{1,0:T(4,128)S(1)} %get-tuple-element.23) | copy-start | bytes 25348
  193.7 10.4 %copy-start.8 = (f32[3,704]{1,0:T(4,128)}, f32[3,704]{1,0:T(4,128)S(1)}, u32[]{:S(2)}) copy-start(f32[3,704]{1,0:T(4,128)S(1)} %get-tuple-element.24) | copy-start | bytes 25348
Sparse Core Ops, SparseCore 0:
  9.6 49.5 all-gather.4
  61.0 57.9 all-gather.2
  122.0 78.6 reduce-scatter.4
  203.4 50.2 reduce-scatter.2
